TPU v7x, 32 devices: a whole 2x2x4 slice. The times are simulated.
32 devices in a mesh: sp: 4 (over y, x), tp: 8 (over z, core).
Axes of the slice: x: 2, y: 2, z: 4, core: 2. Of those that a mesh axis runs over, the one named last changes fastest.
Arguments:
- skip_stream_entry: bfloat16 [2048, 2048], P(('sp', 'tp')), may hold values from -6 to 6
- result_switch_mapped: bfloat16 [2048, 4096], P('sp', 'tp'), may hold values from -6 to 6
- channel_feed_mapped: bfloat16 [2048, 4096], P('sp', 'tp'), may hold values from -6 to 6
- write_coefficient_mapped: bfloat16 [2048, 2048], P('sp', 'tp'), may hold values from -6 to 6
- emission_coefficient_mapped: bfloat16 [2048, 2048], P('sp', 'tp'), may hold values from -6 to 6
- channel_feed_taps: bfloat16 [5, 4096], P(None, 'tp'), may hold values from -2.5 to 2.5
- write_coefficient_taps: bfloat16 [5, 2048], P(None, 'tp'), may hold values from -2.5 to 2.5
- emission_coefficient_taps: bfloat16 [5, 2048], P(None, 'tp'), may hold values from -2.5 to 2.5
- raw_increments: bfloat16 [2, 64, 2048], P(None, 'tp', 'sp'), may hold values from -6 to 6
- channel_log_fade_speed: float32 [2, 64], P(None, 'tp'), may hold values from -20 to 0
- extra_log_fade: float32 [2, 64, 2048], P(None, 'tp', 'sp'), may hold values from -1 to 0
- cluster_scaling_factor: float32 [4096], P('tp'), may hold values from 0.1 to 1.9
- blend_result_matrix: bfloat16 [4096, 2048], P('tp'), may hold values from -0.09375 to 0.09375
- routing_scaling_factor: float32 [2048], replicated, may hold values from 0.1 to 1.9
- specialist_switch_matrix: bfloat16 [8, 2048, 4096], P('sp', None, 'tp'), may hold values from -0.125 to 0.125
- specialist_widen_matrix: bfloat16 [8, 2048, 4096], P('sp', None, 'tp'), may hold values from -0.125 to 0.125
- specialist_contract_matrix: bfloat16 [8, 4096, 2048], P('sp', 'tp'), may hold values from -0.1875 to 0.1875
- picked_specialists: int32 [2048, 2], P(('sp', 'tp')), may hold values from 0 to 7, all different within a row; in each aligned block of 64 rows (0 to 63, 64 to 127, ...) at most 24 rows name the same one
- router_affinities: float32 [2048, 2], P(('sp', 'tp')), may hold values from 0.1 to 1
Outputs:
- result: bfloat16 [2048, 2048], P(('sp', 'tp'))
Inputs may be any that keep to these rules, and one draw needn't show every extreme that they name: `picked_specialists`: each row names 2 different experts. Within the rows of one device (aligned blocks of 64 rows) no expert is named more than 24 times, a bound that some block reaches.
All inputs are finite; a program needn't handle non-finite values.
Results may differ from a plain program's by a relative error of at most 0.02.
Values may be sent and summed in bfloat16 or wider, within the bound.
A program may use at most 64 MiB of HBM per device.

v0:
```python
import functools

import jax
import jax.numpy as jnp
from jax import lax
from jax.experimental import pallas as pl
from jax.experimental.pallas import tpu as pltpu
from jax.sharding import PartitionSpec as P

WIDTH = 2048
HEAD_DIM = 64
GROUPS = 16
STATE = 128
CONV_W = 5
BLOCK = 128
TOP = 2
INNER = 4096


EPSILON = 1e-06
HIGHEST_MODE = lax.Precision.HIGHEST


MESH_IDS = pl.DeviceIdType.MESH
RIM = 8
EDGE = 16


def spread_heads(columns, per_group):
    rows = columns.shape[0]
    lane = lax.broadcasted_iota(jnp.int32, (rows, per_group * HEAD_DIM), 1) // HEAD_DIM
    out = jnp.broadcast_to(columns[:, 0:1], lane.shape)
    for head in range(1, per_group):
        out = jnp.where(lane == head, jnp.broadcast_to(columns[:, head : head + 1], lane.shape), out)
    return out


def silu(value):
    return value * jax.nn.sigmoid(value)


def conv_block(scratch, taps, block, lanes):
    rim = taps.shape[0] // 2
    total = None
    for offset in range(taps.shape[0]):
        start = RIM - rim + offset + block * BLOCK
        term = taps[offset : offset + 1, lanes].astype(jnp.float32) * scratch[start : start + BLOCK, lanes]
        total = term if total is None else total + term
    return silu(total)


def flip(index, mask, count):
    out, bit = index, 1
    while bit < count:
        out = out + ((mask // bit) % 2) * (1 - 2 * ((index // bit) % 2)) * bit
        bit = 2 * bit
    return out


def remote(source, target, send_sem, recv_sem, where):
    return pltpu.make_async_remote_copy(
        src_ref=source, dst_ref=target, send_sem=send_sem, recv_sem=recv_sem,
        device_id=where, device_id_type=MESH_IDS,
    )


def greet(places):
    barrier = pltpu.get_barrier_semaphore()
    for place in places:
        pl.semaphore_signal(barrier, inc=1, device_id=place, device_id_type=MESH_IDS)
    pl.semaphore_wait(barrier, len(places))


def write_route(picks_ref, affinity_ref, route_scr, experts_here, share):
    owned = picks_ref.shape[0]
    peers, core = lax.axis_size("sp"), lax.axis_index("tp") % 2
    picks, affinity = picks_ref[...], affinity_ref[...]
    lane = lax.broadcasted_iota(jnp.int32, (owned, 128), 1)
    marks = [jnp.where(picks[:, k : k + 1] == lane, 1.0, 0.0) for k in range(TOP)]
    earlier = jnp.where(
        lax.broadcasted_iota(jnp.int32, (owned, owned), 0)
        > lax.broadcasted_iota(jnp.int32, (owned, owned), 1),
        1.0,
        0.0,
    ).astype(jnp.bfloat16)
    ahead = jnp.dot(
        earlier, (marks[0] + marks[1]).astype(jnp.bfloat16), preferred_element_type=jnp.float32
    )
    base = (lane % experts_here) * (peers * share) + (lane // experts_here) * share
    base = (base + core * (share // 2)).astype(jnp.float32) + ahead
    places = [jnp.sum(mark * base, axis=1, keepdims=True) for mark in marks]
    whole = affinity[:, 0:1] + affinity[:, 1:2]
    lines = jnp.where(
        lane == 0,
        places[0],
        jnp.where(
            lane == 1,
            places[1],
            jnp.where(
                lane == 2,
                affinity[:, 0:1] / whole,
                jnp.where(lane == 3, affinity[:, 1:2] / whole, 0.0),
            ),
        ),
    )
    blank = jnp.zeros_like(lines)
    rest = [] if 2 * owned == 128 else [jnp.zeros((128 - 2 * owned, 128), jnp.float32)]
    both = jnp.concatenate(
        [jnp.where(core == 0, lines, blank), jnp.where(core == 0, blank, lines)] + rest, axis=0
    )
    route_scr[...] = jnp.transpose(both)[0:8, :]


def mixer_part(
    x_ref, b_ref, c_ref, x_taps, b_taps, c_taps, inc_ref, speed_ref, extra_ref, picks_ref,
    affinity_ref, gain_ref, norm_gain_ref, gate_ref, skip_ref, weight_ref, loads, after_ref,
    normed_ref, routes, experts_here, share,
    x_pad, b_pad, c_pad, x_low, b_low, c_low, x_high, b_high, c_high, fade_scr, x_kept, b_kept,
    c_kept, cum_scr, col_scr, entry_scr, state_ref, target, y_ref, reach_ref, carry_scr, route_scr,
    full_scr, mine_scr, give, take, ship, land,
    edge_send, edge_recv, state_send, state_recv, route_send, route_recv,
    give_send, take_recv, ship_send, land_recv,
):
    count, inner_here = x_ref.shape
    groups = b_ref.shape[1] // STATE
    width = inner_here // groups
    per_group = width // HEAD_DIM
    rows = 2 * per_group
    blocks = count // BLOCK
    rim = x_taps.shape[0] // 2
    here, peers = lax.axis_index("sp"), lax.axis_size("sp")
    seat, seats = lax.axis_index("tp"), lax.axis_size("tp")
    levels = seats // 2
    core, level = seat % 2, seat // 2
    owned, features = skip_ref.shape
    partner = {"tp": seat + 1 - 2 * core}

    edges = []
    for index, (source, low, high) in enumerate(
        ((x_ref, x_low, x_high), (b_ref, b_low, b_high), (c_ref, c_low, c_high))
    ):
        onward = remote(
            source.at[pl.ds(count - EDGE, EDGE)], low, edge_send.at[0, index],
            edge_recv.at[0, index], {"sp": lax.rem(here + 1, peers)},
        )
        back = remote(
            source.at[pl.ds(0, EDGE)], high, edge_send.at[1, index],
            edge_recv.at[1, index], {"sp": lax.rem(here + peers - 1, peers)},
        )
        edges.append((onward, back))

    @pl.when(here < peers - 1)
    def _():
        for onward, _ in edges:
            onward.start()

    @pl.when(here > 0)
    def _():
        for _, back in edges:
            back.start()

    write_route(picks_ref, affinity_ref, route_scr, experts_here, share)
    route_copies = [
        remote(
            route_scr, routes.at[seat], route_send.at[away - 1], route_recv.at[away - 1],
            {"tp": lax.rem(seat + away, seats)},
        )
        for away in range(1, seats)
    ]
    for copy in route_copies:
        copy.start()
    routes[seat] = route_scr[...]
    target[here] = jnp.zeros(target.shape[1:], target.dtype)

    heads = inc_ref.shape[1]
    square_at = [lax.broadcasted_iota(jnp.int32, (heads, heads), axis) for axis in range(2)]
    for first in range(2):
        raw = inc_ref[first].astype(jnp.float32)
        step = jnp.maximum(raw, 0.0) + jnp.log1p(jnp.exp(-jnp.abs(raw)))
        line = jnp.broadcast_to(speed_ref[first : first + 1, :], (heads, heads))
        speed = jnp.sum(
            jnp.where(square_at[0] == square_at[1], jnp.exp(line), 0.0), axis=1, keepdims=True
        )
        fade = -step * speed + extra_ref[first]
        for group in range(groups):
            mine = slice(group * per_group, (group + 1) * per_group)
            spot = first * per_group
            fade_scr[group, spot : spot + per_group, :] = fade[mine, :]
            fade_scr[group, rows + spot : rows + spot + per_group, :] = step[mine, :]
    for pad, source in ((x_pad, x_ref), (b_pad, b_ref), (c_pad, c_ref)):
        pad[RIM : RIM + count, :] = source[...].astype(jnp.float32)

    @pl.when(here > 0)
    def _():
        for onward, _ in edges:
            onward.wait_recv()
        for pad, low in ((x_pad, x_low), (b_pad, b_low), (c_pad, c_low)):
            pad[RIM - rim : RIM, :] = low[...].astype(jnp.float32)[EDGE - rim : EDGE, :]

    @pl.when(here == 0)
    def _():
        for pad in (x_pad, b_pad, c_pad):
            pad[RIM - rim : RIM, :] = jnp.zeros((rim, pad.shape[1]), jnp.float32)

    @pl.when(here < peers - 1)
    def _():
        for _, back in edges:
            back.wait_recv()
        for pad, high in ((x_pad, x_high), (b_pad, b_high), (c_pad, c_high)):
            pad[RIM + count : RIM + count + rim, :] = high[...].astype(jnp.float32)[0:rim, :]

    @pl.when(here == peers - 1)
    def _():
        for pad in (x_pad, b_pad, c_pad):
            pad[RIM + count : RIM + count + rim, :] = jnp.zeros((rim, pad.shape[1]), jnp.float32)

    i_at = lax.broadcasted_iota(jnp.int32, (BLOCK, BLOCK), 0)
    j_at = lax.broadcasted_iota(jnp.int32, (BLOCK, BLOCK), 1)
    up_to = (i_at <= j_at).astype(jnp.float32)
    from_on = (i_at >= j_at).astype(jnp.float32)
    row_at = lax.broadcasted_iota(jnp.int32, (rows, BLOCK), 0)
    col_at = lax.broadcasted_iota(jnp.int32, (1, rows), 1)
    half_lane = lax.broadcasted_iota(jnp.int32, (BLOCK, 2 * HEAD_DIM), 1) < HEAD_DIM

    def state_copy(group, away):
        peer = lax.rem(here + away, peers)
        return remote(
            state_ref.at[jnp.where(peer > here, 0, 1), group], target.at[here, group],
            state_send.at[group, away - 1], state_recv.at[group, away - 1], {"sp": peer},
        )

    all_totals = []
    for group in range(groups):
        lanes_x = slice(group * width, (group + 1) * width)
        lanes_s = slice(group * STATE, (group + 1) * STATE)
        totals, parts = [], []
        for block in range(blocks):
            at = slice(block * BLOCK, (block + 1) * BLOCK)
            fade = fade_scr[group, 0:rows, at]
            step = fade_scr[group, rows : 2 * rows, at]
            onward = jnp.dot(fade, up_to, precision=HIGHEST_MODE, preferred_element_type=jnp.float32)
            back = jnp.dot(fade, from_on, precision=HIGHEST_MODE, preferred_element_type=jnp.float32)
            cum = jnp.where(row_at < per_group, onward, back)
            stacked = jnp.concatenate(
                [cum, step, jnp.zeros((BLOCK - 2 * rows, BLOCK), jnp.float32)], axis=0
            )
            turned = jnp.transpose(stacked)
            cum_col, step_col = turned[:, 0:rows], turned[:, rows : 2 * rows]
            total = jnp.where(col_at < per_group, cum_col[BLOCK - 1 : BLOCK, :], cum_col[0:1, :])
            to_end = jnp.exp(total - cum_col) * step_col
            cum_scr[group, block] = cum
            col_scr[group, block] = cum_col
            x = conv_block(x_pad, x_taps, block, lanes_x)
            b = conv_block(b_pad, b_taps, block, lanes_s)
            x_kept[at, lanes_x] = x
            b_turned = jnp.transpose(b).astype(jnp.bfloat16)
            b_kept[group, block] = b_turned
            weighted = jnp.concatenate(
                [
                    x * spread_heads(to_end[:, 0:per_group], per_group),
                    x * spread_heads(to_end[:, per_group:rows], per_group),
                ],
                axis=1,
            ).astype(jnp.bfloat16)
            parts.append(jnp.dot(b_turned, weighted, preferred_element_type=jnp.float32))
            totals.append(total)
        for first, order in ((0, range(blocks)), (1, range(blocks - 1, -1, -1))):
            lanes = slice(first * width, (first + 1) * width)
            held = jnp.zeros((STATE, width), jnp.float32)
            for block in order:
                entry_scr[group, block, :, lanes] = held.astype(jnp.bfloat16)
                factor = spread_heads(
                    jnp.exp(totals[block][:, first * per_group : (first + 1) * per_group]), per_group
                )
                held = held * factor + parts[block][:, lanes]
            state_ref[first, group, 0:STATE, :] = held.astype(jnp.bfloat16)
            whole = totals[0]
            for block in range(1, blocks):
                whole = whole + totals[block]
            whole = spread_heads(
                jnp.exp(whole[:, first * per_group : (first + 1) * per_group]), per_group
            )
            state_ref[first, group, STATE:, :] = jnp.broadcast_to(
                whole, (state_ref.shape[2] - STATE, width)
            ).astype(jnp.bfloat16)
        for away in range(1, peers):
            state_copy(group, away).start()
        all_totals.append(totals)

    for group in range(groups):
        lanes_x = slice(group * width, (group + 1) * width)
        lanes_s = slice(group * STATE, (group + 1) * STATE)
        totals = all_totals[group]
        for block in range(blocks):
            at = slice(block * BLOCK, (block + 1) * BLOCK)
            step = fade_scr[group, rows : 2 * rows, at]
            cum, cum_col = cum_scr[group, block], col_scr[group, block]
            x = x_kept[at, lanes_x]
            c = conv_block(c_pad, c_taps, block, lanes_s).astype(jnp.bfloat16)
            c_kept[at, lanes_s] = c
            inner = jnp.dot(c, b_kept[group, block], preferred_element_type=jnp.float32)
            mixing = []
            for head in range(per_group):
                other = per_group + head
                gap = jnp.where(
                    i_at >= j_at,
                    cum_col[:, head : head + 1] - cum[head : head + 1, :],
                    cum_col[:, other : other + 1] - cum[other : other + 1, :],
                )
                own, opposite = step[head : head + 1, :], step[other : other + 1, :]
                amount = jnp.where(
                    i_at > j_at, own, jnp.where(i_at < j_at, opposite, own + opposite)
                )
                mixing.append((jnp.exp(gap) * amount * inner).astype(jnp.bfloat16))
            pieces = []
            for pair in range(per_group // 2):
                x_pair = x[:, pair * 2 * HEAD_DIM : (pair + 1) * 2 * HEAD_DIM]
                both = jnp.concatenate(
                    [jnp.where(half_lane, x_pair, 0.0), jnp.where(half_lane, 0.0, x_pair)], axis=0
                ).astype(jnp.bfloat16)
                left = jnp.concatenate([mixing[2 * pair], mixing[2 * pair + 1]], axis=1)
                pieces.append(jnp.dot(left, both, preferred_element_type=jnp.float32))
            readout = jnp.dot(c, entry_scr[group, block], preferred_element_type=jnp.float32)
            fade_in = jnp.exp(cum_col)
            y_ref[at, lanes_x] = (
                jnp.concatenate(pieces, axis=1)
                + readout[:, :width] * spread_heads(fade_in[:, 0:per_group], per_group)
                + readout[:, width:] * spread_heads(fade_in[:, per_group:rows], per_group)
            )
            offset = jnp.zeros((1, rows), jnp.float32)
            for earlier in range(blocks):
                if earlier < block:
                    offset = offset + jnp.where(col_at < per_group, totals[earlier], 0.0)
                if earlier > block:
                    offset = offset + jnp.where(col_at < per_group, 0.0, totals[earlier])
            reach_ref[group, at, :] = jnp.exp(cum_col + offset)

    def at_level(mask):
        return {"tp": 2 * flip(level, mask, levels) + core}

    def hand(mask):
        return remote(give.at[mask], take.at[mask], give_send.at[mask], take_recv.at[mask], partner)

    def post(mask):
        return remote(
            ship.at[mask], land.at[mask], ship_send.at[mask], land_recv.at[mask], at_level(mask)
        )

    for load in loads:
        load.wait()
    for group in range(groups):
        for away in range(1, peers):
            state_copy(group, away).wait_recv()
        for first in range(2):
            held = jnp.zeros((STATE, width), jnp.float32)
            order = range(peers) if first == 0 else range(peers - 1, -1, -1)
            for peer in order:
                fresh = target[peer, group, 0:STATE, :].astype(jnp.float32)
                factor = target[peer, group, STATE : STATE + 1, :].astype(jnp.float32)
                reached = peer < here if first == 0 else peer > here
                held = jnp.where(reached, held * factor + fresh, held)
            carry_scr[group, :, first * width : (first + 1) * width] = held.astype(jnp.bfloat16)

    def pass_on(mask):
        hand(mask).wait_recv()
        ship[mask] = (mine_scr[mask] + take[mask].astype(jnp.float32)).astype(jnp.bfloat16)
        post(mask).start()

    def one_block(turn, _):
        mask = levels - 1 - turn
        at = pl.ds(pl.multiple_of(flip(level, mask, levels) * (2 * owned), 2 * owned), 2 * owned)
        mixed = []
        for group in range(groups):
            lanes = slice(group * width, (group + 1) * width)
            c = c_kept[at, group * STATE : (group + 1) * STATE]
            readout = jnp.dot(c, carry_scr[group], preferred_element_type=jnp.float32)
            reach = reach_ref[group, at, :]
            y = (
                y_ref[at, lanes]
                + readout[:, :width] * spread_heads(reach[:, 0:per_group], per_group)
                + readout[:, width:] * spread_heads(reach[:, per_group:rows], per_group)
            )
            gated = y * silu(gate_ref[at, lanes].astype(jnp.float32))
            square = jnp.mean(gated * gated, axis=-1, keepdims=True)
            mixed.append(
                (gated * lax.rsqrt(square + EPSILON) * gain_ref[:, lanes]).astype(jnp.bfloat16)
            )
        rows_mixed = mixed[0] if groups == 1 else jnp.concatenate(mixed, axis=1)
        tile = min(512, features)
        for start in range(0, features, tile):
            full_scr[:, start : start + tile] = jnp.dot(
                rows_mixed, weight_ref[:, start : start + tile], preferred_element_type=jnp.float32
            )
        own = pl.multiple_of(core * owned, owned)
        other = pl.multiple_of((1 - core) * owned, owned)
        give[mask] = full_scr[pl.ds(other, owned), :].astype(jnp.bfloat16)
        hand(mask).start()
        mine_scr[mask] = full_scr[pl.ds(own, owned), :]

        @pl.when(turn > 0)
        def _():
            pass_on(mask + 1)

        return 0

    lax.fori_loop(0, levels, one_block, 0)
    hand(0).wait_recv()
    total = mine_scr[0] + take[0].astype(jnp.float32)
    for mask in range(1, levels):
        post(mask).wait_recv()
        total = total + land[mask].astype(jnp.float32)
    after = (skip_ref[...].astype(jnp.float32) + total).astype(jnp.bfloat16)
    after_ref[...] = after
    values = after.astype(jnp.float32)
    scale = lax.rsqrt(jnp.mean(values * values, axis=-1, keepdims=True) + EPSILON)
    normed_ref[...] = (values * scale * norm_gain_ref[...]).astype(jnp.bfloat16)
    for copy in route_copies:
        copy.wait_recv()

    def settle():
        for mask in range(levels):
            hand(mask).wait_send()
            if mask:
                post(mask).wait_send()
        for copy in route_copies:
            copy.wait_send()
        for group in range(groups):
            for away in range(1, peers):
                state_copy(group, away).wait_send()

        @pl.when(here < peers - 1)
        def _():
            for onward, _ in edges:
                onward.wait_send()

        @pl.when(here > 0)
        def _():
            for _, back in edges:
                back.wait_send()

    return settle


AHEAD = 2


def experts_part(
    normed_ref, after_ref, routes_ref, out_ref, loads, settle,
    rows_scr, stage, own_in, other_in, other_out, other_got, kept, hidden, returned,
    full_scr, mine_scr, give, take, ship, land, gate_w, up_w, down_w,
    row_send, row_recv, pair_send, pair_recv, out_send, out_recv, side_send, side_recv,
    sum_send, sum_recv, back_send, back_recv, give_send, take_recv, ship_send, land_recv,
):
    here, peers = lax.axis_index("sp"), lax.axis_size("sp")
    seat = lax.axis_index("tp")
    levels = lax.axis_size("tp") // 2
    core, level = seat % 2, seat // 2
    owned, features = normed_ref.shape
    share = stage.shape[2]
    slots = peers * share
    tokens = 2 * owned
    partner = {"tp": seat + 1 - 2 * core}
    away_order = list(range(peers - 1, 0, -1))

    def floor_of(mask):
        return flip(level, mask, levels)

    def at_level(mask):
        return {"tp": 2 * floor_of(mask) + core}

    def column(away):
        return flip(here, away, peers)

    def row_copy(mask):
        return remote(
            normed_ref, rows_scr.at[level, core], row_send.at[mask], row_recv.at[mask],
            at_level(mask),
        )

    def pair_copy(mask):
        spot = rows_scr.at[floor_of(mask), core]
        source = normed_ref if isinstance(mask, int) and mask == 0 else spot
        return remote(source, spot, pair_send.at[mask], pair_recv.at[mask], partner)

    def out_copy(mask, away):
        floor = floor_of(mask)
        return remote(
            stage.at[floor, column(away)], own_in.at[floor, here],
            out_send.at[mask, away], out_recv.at[mask, away], {"sp": column(away)},
        )

    def side_copy(mask, away):
        return remote(
            own_in.at[floor_of(mask), column(away)], other_in.at[mask % 2, column(away)],
            side_send.at[mask, away], side_recv.at[mask, away], partner,
        )

    def sum_copy(mask):
        return remote(
            other_out.at[mask % 2], other_got.at[mask % 2], sum_send.at[mask], sum_recv.at[mask],
            partner,
        )

    def back_copy(mask, away):
        floor = floor_of(mask)
        return remote(
            stage.at[floor, column(away)], returned.at[floor, here],
            back_send.at[mask, away], back_recv.at[mask, away], {"sp": column(away)},
        )

    def hand(mask):
        return remote(give.at[mask], take.at[mask], give_send.at[mask], take_recv.at[mask], partner)

    def post(mask):
        return remote(
            ship.at[mask], land.at[mask], ship_send.at[mask], land_recv.at[mask], at_level(mask)
        )

    rows_scr[level, core] = normed_ref[...]
    for mask in range(1, levels):
        row_copy(mask).start()

    def routes_of(mask):
        floor = floor_of(mask)
        return routes_ref[2 * floor] + routes_ref[2 * floor + 1]

    def dispatch(mask):
        floor = floor_of(mask)
        pair_copy(mask).start()
        tile = routes_of(mask)
        code = (
            lax.broadcasted_iota(jnp.int32, (slots, tokens), 0) + core * slots
        ).astype(jnp.float32)
        chosen = (tile[0:1, 0:tokens] == code) | (tile[1:2, 0:tokens] == code)
        chosen = jnp.where(chosen, 1.0, 0.0).astype(jnp.bfloat16)
        pair_copy(mask).wait_recv()
        width = min(512, features)
        for start in range(0, features, width):
            lanes = slice(start, start + width)
            rows = rows_scr[floor, :, :, lanes].reshape(tokens, width)
            picked = jnp.dot(chosen, rows, preferred_element_type=jnp.float32)
            stage[floor, :, :, lanes] = picked.astype(jnp.bfloat16).reshape(peers, share, width)
        own_in[floor, here] = stage[floor, here]
        for away in away_order:
            out_copy(mask, away).start()

    def arrive_and_dispatch(mask):
        row_copy(mask).wait_recv()
        dispatch(mask)

    dispatch(0)
    for mask in range(1, min(AHEAD, levels)):
        arrive_and_dispatch(mask)
    for load in loads:
        load.wait()

    def expert(index, source, store):
        hid = gate_w.shape[2]
        width = min(256, hid)

        def up_tile(n, _):
            lanes = pl.ds(pl.multiple_of(n * width, width), width)
            x = source[...].reshape(slots, features)
            gate = jnp.dot(x, gate_w[index, :, lanes], preferred_element_type=jnp.float32)
            up = jnp.dot(x, up_w[index, :, lanes], preferred_element_type=jnp.float32)
            hidden[:, lanes] = (silu(gate) * up).astype(jnp.bfloat16)
            return 0

        lax.fori_loop(0, hid // width, up_tile, 0)
        wide = min(512, features)

        def down_tile(n, _):
            lanes = pl.ds(pl.multiple_of(n * wide, wide), wide)
            store(
                lanes,
                jnp.dot(hidden[...], down_w[index, :, lanes], preferred_element_type=jnp.float32),
            )
            return 0

        lax.fori_loop(0, features // wide, down_tile, 0)

    def one_floor(mask, _):
        floor = floor_of(mask)
        side_copy(mask, 0).start()
        for away in away_order:
            out_copy(mask, away).wait_recv()
            side_copy(mask, away).start()
        if AHEAD < levels:

            @pl.when(mask + AHEAD < levels)
            def _():
                arrive_and_dispatch(mask + AHEAD)

        for away in range(peers):
            side_copy(mask, away).wait_recv()

        @pl.when(mask >= 2)
        def _():
            sum_copy(mask - 2).wait_send()

        def give_out(lanes, value):
            other_out[mask % 2, :, lanes] = value.astype(jnp.bfloat16)

        def keep(lanes, value):
            kept[:, lanes] = value

        expert(1 - core, other_in.at[mask % 2], give_out)
        sum_copy(mask).start()
        expert(core, own_in.at[floor], keep)
        for away in away_order:
            out_copy(mask, away).wait_send()
        sum_copy(mask).wait_recv()
        both = (kept[...] + other_got[mask % 2].astype(jnp.float32)).astype(jnp.bfloat16)
        stage[floor] = both.reshape(peers, share, features)
        returned[floor, here] = stage[floor, here]

        @pl.when(mask > 0)
        def _():
            for away in away_order:
                back_copy(mask, away).start()

        return 0

    lax.fori_loop(0, levels, one_floor, 0)
    for away in away_order:
        back_copy(0, away).start()

    def pass_on(mask):
        hand(mask).wait_recv()
        ship[mask] = (mine_scr[mask] + take[mask].astype(jnp.float32)).astype(jnp.bfloat16)
        post(mask).start()

    def combine(turn, _):
        mask = (turn + 1) % levels
        tile = routes_of(mask)
        size = tile.shape[1]
        turned = jnp.transpose(
            jnp.concatenate([tile, jnp.zeros((size - tile.shape[0], size), jnp.float32)], axis=0)
        )[0:tokens, :]
        code = (
            lax.broadcasted_iota(jnp.int32, (tokens, slots), 1) + core * slots
        ).astype(jnp.float32)
        weight = jnp.where(turned[:, 0:1] == code, turned[:, 2:3], 0.0) + jnp.where(
            turned[:, 1:2] == code, turned[:, 3:4], 0.0
        )
        high = weight.astype(jnp.bfloat16)
        low = (weight - high.astype(jnp.float32)).astype(jnp.bfloat16)
        for away in away_order:
            back_copy(mask, away).wait_recv()
        width = min(512, features)
        for start in range(0, features, width):
            lanes = slice(start, start + width)
            got = returned[floor_of(mask), :, :, lanes].reshape(slots, width)
            full_scr[:, lanes] = jnp.dot(
                high, got, preferred_element_type=jnp.float32
            ) + jnp.dot(low, got, preferred_element_type=jnp.float32)
        own = pl.multiple_of(core * owned, owned)
        other = pl.multiple_of((1 - core) * owned, owned)
        give[mask] = full_scr[pl.ds(other, owned), :].astype(jnp.bfloat16)
        hand(mask).start()
        mine_scr[mask] = full_scr[pl.ds(own, owned), :]

        @pl.when(turn > 0)
        def _():
            pass_on(turn)

        return 0

    settle()
    lax.fori_loop(0, levels, combine, 0)
    hand(0).wait_recv()
    total = mine_scr[0] + take[0].astype(jnp.float32)
    for mask in range(1, levels):
        post(mask).wait_recv()
        total = total + land[mask].astype(jnp.float32)
    out_ref[...] = (after_ref[...].astype(jnp.float32) + total).astype(jnp.bfloat16)

    for mask in range(levels):
        pair_copy(mask).wait_send()
        hand(mask).wait_send()
        if mask:
            row_copy(mask).wait_send()
            post(mask).wait_send()
        if mask + 2 >= levels:
            sum_copy(mask).wait_send()
        for away in range(peers):
            side_copy(mask, away).wait_send()
            if away:
                back_copy(mask, away).wait_send()


def layer_kernel(experts_here, share, counts, *refs):
    refs = list(refs)

    def take(number):
        out = refs[:number]
        del refs[:number]
        return out

    near = take(counts[0])
    far = take(counts[1])
    (out_ref,) = take(1)
    loaded = take(counts[1])
    after_ref, normed_ref, routes = take(3)
    mixer_own = take(counts[2])
    shared = take(6)
    mixer_flags = take(10)
    experts_own = take(9)
    experts_flags = take(16)
    (load_sem,) = take(1)
    loads = [
        pltpu.make_async_copy(source, target, load_sem.at[index])
        for index, (source, target) in enumerate(zip(far, loaded))
    ]
    for load in loads:
        load.start()
    here, peers = lax.axis_index("sp"), lax.axis_size("sp")
    seat, seats = lax.axis_index("tp"), lax.axis_size("tp")
    greet(
        [{"sp": lax.rem(here + away, peers)} for away in range(1, peers)]
        + [{"tp": lax.rem(seat + away, seats)} for away in range(1, seats)]
    )
    settle = mixer_part(
        *near, *loaded[0:3], loads[0:3], after_ref, normed_ref, routes, experts_here, share,
        *mixer_own, *shared, *mixer_flags,
    )
    experts_part(
        normed_ref, after_ref, routes, out_ref, loads[3:], settle,
        *experts_own, *shared, *loaded[3:], *experts_flags,
    )


def per_device(
    skip_stream_entry,
    result_switch_mapped,
    channel_feed_mapped,
    write_coefficient_mapped,
    emission_coefficient_mapped,
    channel_feed_taps,
    write_coefficient_taps,
    emission_coefficient_taps,
    raw_increments,
    channel_log_fade_speed,
    extra_log_fade,
    cluster_scaling_factor,
    blend_result_matrix,
    routing_scaling_factor,
    specialist_switch_matrix,
    specialist_widen_matrix,
    specialist_contract_matrix,
    picked_specialists,
    router_affinities,
):
    count, inner_here = channel_feed_mapped.shape
    owned, features = skip_stream_entry.shape
    experts_here, _, units = specialist_switch_matrix.shape
    peers, seats = lax.axis_size("sp"), lax.axis_size("tp")
    levels = seats // 2
    groups = write_coefficient_mapped.shape[1] // STATE
    width = inner_here // groups
    rows = 2 * (width // HEAD_DIM)
    blocks = count // BLOCK
    depth = STATE + 16
    capacity = max(2, 3 * TOP * owned // (2 * experts_here * peers))
    share = 2 * (-(-capacity // 8) * 8)
    slots = peers * share
    vmem, anywhere = pl.BlockSpec(memory_space=pltpu.VMEM), pl.BlockSpec(memory_space=pl.ANY)

    def half(*shape):
        return pltpu.VMEM(shape, jnp.bfloat16)

    def full(*shape):
        return pltpu.VMEM(shape, jnp.float32)

    def flags(*shape):
        return pltpu.SemaphoreType.DMA(shape)

    near = [
        channel_feed_mapped, write_coefficient_mapped, emission_coefficient_mapped,
        channel_feed_taps, write_coefficient_taps, emission_coefficient_taps, raw_increments,
        channel_log_fade_speed, extra_log_fade, picked_specialists, router_affinities,
        cluster_scaling_factor.reshape(1, -1), routing_scaling_factor.reshape(1, -1),
    ]
    far = [
        result_switch_mapped, skip_stream_entry, blend_result_matrix,
        specialist_switch_matrix, specialist_widen_matrix, specialist_contract_matrix,
    ]
    lines = groups * STATE
    mixer_own = [
        full(count + 2 * RIM, inner_here), full(count + 2 * RIM, lines), full(count + 2 * RIM, lines),
        half(EDGE, inner_here), half(EDGE, lines), half(EDGE, lines),
        half(EDGE, inner_here), half(EDGE, lines), half(EDGE, lines),
        full(groups, 2 * rows, count), full(count, inner_here), half(groups, blocks, STATE, BLOCK),
        half(count, lines), full(groups, blocks, rows, BLOCK), full(groups, blocks, BLOCK, rows),
        half(groups, blocks, STATE, 2 * width), half(2, groups, depth, width),
        half(peers, groups, depth, width), full(count, inner_here), full(groups, count, rows),
        half(groups, STATE, 2 * width), full(8, 128),
    ]
    slab = (levels, owned, features)
    shared = [full(2 * owned, features), full(*slab)] + [half(*slab)] * 4
    mixer_flags = [
        flags(2, 3), flags(2, 3), flags(groups, peers - 1), flags(groups, peers - 1),
        flags(seats - 1), flags(seats - 1), flags(levels), flags(levels), flags(levels), flags(levels),
    ]
    experts_own = [
        half(levels, 2, owned, features),
        half(levels, peers, share, features),
        half(levels, peers, share, features),
        half(2, peers, share, features),
        half(2, slots, features),
        half(2, slots, features),
        full(slots, features),
        half(slots, units),
        half(levels, peers, share, features),
    ]
    experts_flags = [
        flags(levels), flags(levels), flags(levels), flags(levels),
        flags(levels, peers), flags(levels, peers), flags(levels, peers), flags(levels, peers),
        flags(levels), flags(levels), flags(levels, peers), flags(levels, peers),
        flags(levels), flags(levels), flags(levels), flags(levels),
    ]
    return pl.pallas_call(
        functools.partial(layer_kernel, experts_here, share, (len(near), len(far), len(mixer_own))),
        in_specs=[vmem] * len(near) + [anywhere] * len(far),
        out_specs=vmem,
        out_shape=jax.ShapeDtypeStruct((owned, features), jnp.bfloat16),
        scratch_shapes=[half(*array.shape) for array in far]
        + [half(owned, features), half(owned, features), full(seats, 8, 128)]
        + mixer_own + shared + mixer_flags + experts_own + experts_flags + [flags(len(far))],
        compiler_params=pltpu.CompilerParams(
            collective_id=0, has_side_effects=True, vmem_limit_bytes=67043328
        ),
        name="layer",
    )(*near, *far)


def solution(mesh):
    in_specs = (
        P(("sp", "tp"), None),
        P("sp", "tp"),
        P("sp", "tp"),
        P("sp", "tp"),
        P("sp", "tp"),
        P(None, "tp"),
        P(None, "tp"),
        P(None, "tp"),
        P(None, "tp", "sp"),
        P(None, "tp"),
        P(None, "tp", "sp"),
        P("tp"),
        P("tp", None),
        P(),
        P("sp", None, "tp"),
        P("sp", None, "tp"),
        P("sp", "tp", None),
        P(("sp", "tp"), None),
        P(("sp", "tp"), None),
    )
    out_specs = P(("sp", "tp"), None)
    return jax.shard_map(
        per_device, mesh=mesh, in_specs=in_specs, out_specs=out_specs, check_vma=False
    )
```

profile of v0, /device:TPU:17, one launch (start us, length us, event | category | flops | bytes accessed | tf_op | source)
XLA Modules:
  0.0 140.6 jit_solution(16064157167010596188)
XLA Ops:
  0.0 1.4 copy.20.refs_9_
  1.4 1.4 copy.21.refs_10_
  2.7 136.2 %layer.1 = bf16[64,2048]{1,0:T(8,128)(2,1)} custom-call(bf16[512,512]{1,0:T(8,128)(2,1)} %refs_0_.1, bf16[512,256]{1,0:T(8,128)(2,1)} %refs_1_.1, bf16[512,256]{1,0:T(8,128)(2,1)} %refs_2_.1, bf16[5,512]{1,0:T(8,128)(2,1)} %refs_3_.1, bf16[5,256]{1,0:T(8,128)(2,1)} %refs_4_.1, bf16[5,256]{1,0:T(8,128)(2,1)} %refs_5_.1, bf16[2,8,512]{2,1,0:T(8,128)(2,1)} %refs_6_.1, ...), custom_call_target="tpu_custom_call" | custom-call | tf_op jit(solution)/shard_map/layer/pallas_call | solution.py:822
  138.9 1.7 %copy.23 = bf16[64,2048]{1,0:T(8,128)(2,1)} copy(bf16[64,2048]{1,0:T(8,128)(2,1)} %layer.1) | data formatting | bytes 524288
where the time goes:
time: 142 us; the launch traced here: 141 us
  Pallas kernels  136 us (96%)
  local copies, waits for them, and re-layouts  4.42 us (3%)
    pallas_call x1, Pallas kernels, per_device(): pl.pallas_call(functools.partial(layer_kernel, experts_here, share, (len(...  136 us
    unnamed x3, local copies, waits for them, and re-layouts  4.42 us

commit v1 on v0

--- a/solution.py
+++ b/solution.py
@@ -57,6 +57,15 @@
     return out
 
 
+def low_bit(mask, count):
+    out, bit = 0, count // 2
+    while bit >= 1:
+        odd = (mask // bit) % 2
+        out = odd * bit + (1 - odd) * out
+        bit = bit // 2
+    return out
+
+
 def remote(source, target, send_sem, recv_sem, where):
     return pltpu.make_async_remote_copy(
         src_ref=source, dst_ref=target, send_sem=send_sem, recv_sem=recv_sem,
@@ -72,43 +81,36 @@
 
 
 def write_route(picks_ref, affinity_ref, route_scr, experts_here, share):
-    owned = picks_ref.shape[0]
+    owned = picks_ref.shape[1]
     peers, core = lax.axis_size("sp"), lax.axis_index("tp") % 2
     picks, affinity = picks_ref[...], affinity_ref[...]
-    lane = lax.broadcasted_iota(jnp.int32, (owned, 128), 1)
-    marks = [jnp.where(picks[:, k : k + 1] == lane, 1.0, 0.0) for k in range(TOP)]
+    count = -(-experts_here * peers // 8) * 8
+    expert = lax.broadcasted_iota(jnp.int32, (count, owned), 0)
+    marks = [jnp.where(picks[k : k + 1, :] == expert, 1.0, 0.0) for k in range(TOP)]
     earlier = jnp.where(
         lax.broadcasted_iota(jnp.int32, (owned, owned), 0)
-        > lax.broadcasted_iota(jnp.int32, (owned, owned), 1),
+        < lax.broadcasted_iota(jnp.int32, (owned, owned), 1),
         1.0,
         0.0,
     ).astype(jnp.bfloat16)
     ahead = jnp.dot(
-        earlier, (marks[0] + marks[1]).astype(jnp.bfloat16), preferred_element_type=jnp.float32
+        (marks[0] + marks[1]).astype(jnp.bfloat16), earlier, preferred_element_type=jnp.float32
     )
-    base = (lane % experts_here) * (peers * share) + (lane // experts_here) * share
+    base = (expert % experts_here) * (peers * share) + (expert // experts_here) * share
     base = (base + core * (share // 2)).astype(jnp.float32) + ahead
-    places = [jnp.sum(mark * base, axis=1, keepdims=True) for mark in marks]
-    whole = affinity[:, 0:1] + affinity[:, 1:2]
-    lines = jnp.where(
-        lane == 0,
-        places[0],
-        jnp.where(
-            lane == 1,
-            places[1],
-            jnp.where(
-                lane == 2,
-                affinity[:, 0:1] / whole,
-                jnp.where(lane == 3, affinity[:, 1:2] / whole, 0.0),
-            ),
-        ),
+    places = [jnp.sum(mark * base, axis=0, keepdims=True) for mark in marks]
+    whole = affinity[0:1, :] + affinity[1:2, :]
+    lines = jnp.concatenate(
+        places
+        + [affinity[0:1, :] / whole, affinity[1:2, :] / whole]
+        + [jnp.zeros((8 - 2 * TOP, owned), jnp.float32)],
+        axis=0,
     )
     blank = jnp.zeros_like(lines)
-    rest = [] if 2 * owned == 128 else [jnp.zeros((128 - 2 * owned, 128), jnp.float32)]
-    both = jnp.concatenate(
-        [jnp.where(core == 0, lines, blank), jnp.where(core == 0, blank, lines)] + rest, axis=0
+    rest = [] if 2 * owned == 128 else [jnp.zeros((8, 128 - 2 * owned), jnp.float32)]
+    route_scr[...] = jnp.concatenate(
+        [jnp.where(core == 0, lines, blank), jnp.where(core == 0, blank, lines)] + rest, axis=1
     )
-    route_scr[...] = jnp.transpose(both)[0:8, :]
 
 
 def mixer_part(
@@ -343,7 +345,8 @@
 
     def post(mask):
         return remote(
-            ship.at[mask], land.at[mask], ship_send.at[mask], land_recv.at[mask], at_level(mask)
+            ship.at[mask], land.at[mask], ship_send.at[mask], land_recv.at[mask],
+            at_level(low_bit(mask, levels)),
         )
 
     for load in loads:
@@ -361,13 +364,20 @@
                 held = jnp.where(reached, held * factor + fresh, held)
             carry_scr[group, :, first * width : (first + 1) * width] = held.astype(jnp.bfloat16)
 
-    def pass_on(mask):
+    def gather(mask, lows):
         hand(mask).wait_recv()
-        ship[mask] = (mine_scr[mask] + take[mask].astype(jnp.float32)).astype(jnp.bfloat16)
+        total = mine_scr[mask] + take[mask].astype(jnp.float32)
+        for low in lows:
+            post(mask + low).wait_recv()
+            total = total + land[mask + low].astype(jnp.float32)
+        return total
+
+    def pass_on(mask, lows):
+        ship[mask] = gather(mask, lows).astype(jnp.bfloat16)
         post(mask).start()
 
     def one_block(turn, _):
-        mask = levels - 1 - turn
+        mask = jnp.where(turn < levels // 2, levels - 1 - 2 * turn, 2 * levels - 2 - 2 * turn)
         at = pl.ds(pl.multiple_of(flip(level, mask, levels) * (2 * owned), 2 * owned), 2 * owned)
         mixed = []
         for group in range(groups):
@@ -397,18 +407,18 @@
         hand(mask).start()
         mine_scr[mask] = full_scr[pl.ds(own, owned), :]
 
-        @pl.when(turn > 0)
+        @pl.when((turn > 0) & (turn <= levels // 2))
         def _():
-            pass_on(mask + 1)
+            pass_on(levels + 1 - 2 * turn, [])
 
         return 0
 
     lax.fori_loop(0, levels, one_block, 0)
-    hand(0).wait_recv()
-    total = mine_scr[0] + take[0].astype(jnp.float32)
-    for mask in range(1, levels):
-        post(mask).wait_recv()
-        total = total + land[mask].astype(jnp.float32)
+    bits = [1 << n for n in range(levels.bit_length() - 1)]
+    for bit in bits[1:]:
+        for mask in range(levels - bit, 0, -2 * bit):
+            pass_on(mask, [low for low in bits if low < bit])
+    total = gather(0, bits)
     after = (skip_ref[...].astype(jnp.float32) + total).astype(jnp.bfloat16)
     after_ref[...] = after
     values = after.astype(jnp.float32)
@@ -614,7 +624,7 @@
         stage[floor] = both.reshape(peers, share, features)
         returned[floor, here] = stage[floor, here]
 
-        @pl.when(mask > 0)
+        @pl.when(mask >= levels // 2)
         def _():
             for away in away_order:
                 back_copy(mask, away).start()
@@ -622,8 +632,12 @@
         return 0
 
     lax.fori_loop(0, levels, one_floor, 0)
-    for away in away_order:
-        back_copy(0, away).start()
+    for mask in range(levels // 2 - 1, -1, -1):
+        for away in away_order:
+            back_copy(mask, away).start()
+
+    def turn_mask(turn):
+        return jnp.where(turn < levels // 2, turn + levels // 2, levels - 1 - turn)
 
     def pass_on(mask):
         hand(mask).wait_recv()
@@ -631,7 +645,7 @@
         post(mask).start()
 
     def combine(turn, _):
-        mask = (turn + 1) % levels
+        mask = turn_mask(turn)
         tile = routes_of(mask)
         size = tile.shape[1]
         turned = jnp.transpose(
@@ -662,7 +676,7 @@
 
         @pl.when(turn > 0)
         def _():
-            pass_on(turn)
+            pass_on(turn_mask(turn - 1))
 
         return 0
 
@@ -673,7 +687,7 @@
     for mask in range(1, levels):
         post(mask).wait_recv()
         total = total + land[mask].astype(jnp.float32)
-    out_ref[...] = (after_ref[...].astype(jnp.float32) + total).astype(jnp.bfloat16)
+    out_ref[...] = after_ref[...].astype(jnp.float32) + total
 
     for mask in range(levels):
         pair_copy(mask).wait_send()
@@ -778,7 +792,7 @@
     near = [
         channel_feed_mapped, write_coefficient_mapped, emission_coefficient_mapped,
         channel_feed_taps, write_coefficient_taps, emission_coefficient_taps, raw_increments,
-        channel_log_fade_speed, extra_log_fade, picked_specialists, router_affinities,
+        channel_log_fade_speed, extra_log_fade, picked_specialists.T, router_affinities.T,
         cluster_scaling_factor.reshape(1, -1), routing_scaling_factor.reshape(1, -1),
     ]
     far = [
@@ -823,7 +837,7 @@
         functools.partial(layer_kernel, experts_here, share, (len(near), len(far), len(mixer_own))),
         in_specs=[vmem] * len(near) + [anywhere] * len(far),
         out_specs=vmem,
-        out_shape=jax.ShapeDtypeStruct((owned, features), jnp.bfloat16),
+        out_shape=jax.ShapeDtypeStruct((owned, features), jnp.float32),
         scratch_shapes=[half(*array.shape) for array in far]
         + [half(owned, features), half(owned, features), full(seats, 8, 128)]
         + mixer_own + shared + mixer_flags + experts_own + experts_flags + [flags(len(far))],
@@ -831,7 +845,7 @@
             collective_id=0, has_side_effects=True, vmem_limit_bytes=67043328
         ),
         name="layer",
-    )(*near, *far)
+    )(*near, *far).astype(jnp.bfloat16)
 
 
 def solution(mesh):

time: 142 us -> 133 us (0.937)
  Pallas kernels: 136 us -> 129 us
  local copies, waits for them, and re-layouts: 4.42 us -> 0 us
  other arithmetic: 0 us -> 1.77 us
    pallas_call x1, Pallas kernels: 136 us -> 129 us  [per_device(): pl.pallas_call(functools.partial(layer_kernel, experts_here, share, (len(...]
    unnamed x3 -> x0, local copies, waits for them, and re-layouts: 4.42 us -> none
    convert_element_type x0 -> x1, other arithmetic: none -> 1.77 us  [per_device(): return pl.pallas_call(functools.partial(layer_kernel, experts_here, share...]
where the time goes in v1:
time: 133 us; the launch traced here: 131 us
  Pallas kernels  129 us (97%)
  other arithmetic  1.77 us (1%)
    pallas_call x1, Pallas kernels, per_device(): pl.pallas_call(functools.partial(layer_kernel, experts_here, share, (len(...  129 us

profile of v1, /device:TPU:17, one launch (start us, length us, event | category | flops | bytes accessed | tf_op | source)
XLA Modules:
  0.0 131.2 jit_solution(9959220350059126505)
XLA Ops:
  0.0 129.4 %layer.1 = f32[64,2048]{1,0:T(8,128)} custom-call(bf16[512,512]{1,0:T(8,128)(2,1)} %refs_0_.1, bf16[512,256]{1,0:T(8,128)(2,1)} %refs_1_.1, bf16[512,256]{1,0:T(8,128)(2,1)} %refs_2_.1, bf16[5,512]{1,0:T(8,128)(2,1)} %refs_3_.1, bf16[5,256]{1,0:T(8,128)(2,1)} %refs_4_.1, bf16[5,256]{1,0:T(8,128)(2,1)} %refs_5_.1, bf16[2,8,512]{2,1,0:T(8,128)(2,1)} %refs_6_.1, ...), custom_call_target="tpu_custom_call" | custom-call | tf_op jit(solution)/shard_map/layer/pallas_call | solution.py:836
  129.5 1.8 %convert_element_type.3 = bf16[64,2048]{1,0:T(8,128)(2,1)} convert(f32[64,2048]{1,0:T(8,128)} %layer.1) | non-fusion elementwise | flops 131072 | bytes 786432 | tf_op jit(solution)/shard_map/convert_element_type | solution.py:848

commit v2 on v1

--- a/solution.py
+++ b/solution.py
@@ -220,7 +220,6 @@
     j_at = lax.broadcasted_iota(jnp.int32, (BLOCK, BLOCK), 1)
     up_to = (i_at <= j_at).astype(jnp.float32)
     from_on = (i_at >= j_at).astype(jnp.float32)
-    row_at = lax.broadcasted_iota(jnp.int32, (rows, BLOCK), 0)
     col_at = lax.broadcasted_iota(jnp.int32, (1, rows), 1)
     half_lane = lax.broadcasted_iota(jnp.int32, (BLOCK, 2 * HEAD_DIM), 1) < HEAD_DIM
 
@@ -230,6 +229,31 @@
             state_ref.at[jnp.where(peer > here, 0, 1), group], target.at[here, group],
             state_send.at[group, away - 1], state_recv.at[group, away - 1], {"sp": peer},
         )
+
+    spots = [(group, block) for group in range(groups) for block in range(blocks)]
+    fades = jnp.concatenate(
+        [fade_scr[g, 0:rows, b * BLOCK : (b + 1) * BLOCK] for g, b in spots], axis=0
+    )
+    onward = jnp.dot(fades, up_to, precision=HIGHEST_MODE, preferred_element_type=jnp.float32)
+    back = jnp.dot(fades, from_on, precision=HIGHEST_MODE, preferred_element_type=jnp.float32)
+    row_at = lax.broadcasted_iota(jnp.int32, fades.shape, 0)
+    sums = jnp.where(row_at % rows < per_group, onward, back)
+    lines, columns, per_turn = [], {}, BLOCK // (2 * rows)
+    for index, (g, b) in enumerate(spots):
+        cum = sums[index * rows : (index + 1) * rows, :]
+        cum_scr[g, b] = cum
+        lines += [cum, fade_scr[g, rows : 2 * rows, b * BLOCK : (b + 1) * BLOCK]]
+    for start in range(0, len(spots), per_turn):
+        part = lines[2 * start : 2 * (start + per_turn)]
+        rest = BLOCK - rows * len(part)
+        if rest:
+            part = part + [jnp.zeros((rest, BLOCK), jnp.float32)]
+        turned = jnp.transpose(jnp.concatenate(part, axis=0))
+        for offset, spot in enumerate(spots[start : start + per_turn]):
+            lane = 2 * rows * offset
+            columns[spot] = (
+                turned[:, lane : lane + rows], turned[:, lane + rows : lane + 2 * rows]
+            )
 
     all_totals = []
     for group in range(groups):
@@ -238,19 +262,9 @@
         totals, parts = [], []
         for block in range(blocks):
             at = slice(block * BLOCK, (block + 1) * BLOCK)
-            fade = fade_scr[group, 0:rows, at]
-            step = fade_scr[group, rows : 2 * rows, at]
-            onward = jnp.dot(fade, up_to, precision=HIGHEST_MODE, preferred_element_type=jnp.float32)
-            back = jnp.dot(fade, from_on, precision=HIGHEST_MODE, preferred_element_type=jnp.float32)
-            cum = jnp.where(row_at < per_group, onward, back)
-            stacked = jnp.concatenate(
-                [cum, step, jnp.zeros((BLOCK - 2 * rows, BLOCK), jnp.float32)], axis=0
-            )
-            turned = jnp.transpose(stacked)
-            cum_col, step_col = turned[:, 0:rows], turned[:, rows : 2 * rows]
+            cum_col, step_col = columns[group, block]
             total = jnp.where(col_at < per_group, cum_col[BLOCK - 1 : BLOCK, :], cum_col[0:1, :])
             to_end = jnp.exp(total - cum_col) * step_col
-            cum_scr[group, block] = cum
             col_scr[group, block] = cum_col
             x = conv_block(x_pad, x_taps, block, lanes_x)
             b = conv_block(b_pad, b_taps, block, lanes_s)
@@ -290,16 +304,28 @@
         all_totals.append(totals)
 
     for group in range(groups):
-        lanes_x = slice(group * width, (group + 1) * width)
         lanes_s = slice(group * STATE, (group + 1) * STATE)
         totals = all_totals[group]
         for block in range(blocks):
             at = slice(block * BLOCK, (block + 1) * BLOCK)
+            c_kept[at, lanes_s] = conv_block(c_pad, c_taps, block, lanes_s).astype(jnp.bfloat16)
+            offset = jnp.zeros((1, rows), jnp.float32)
+            for earlier in range(blocks):
+                if earlier < block:
+                    offset = offset + jnp.where(col_at < per_group, totals[earlier], 0.0)
+                if earlier > block:
+                    offset = offset + jnp.where(col_at < per_group, 0.0, totals[earlier])
+            reach_ref[group, at, :] = jnp.exp(col_scr[group, block] + offset)
+
+    def within(block):
+        at = pl.ds(pl.multiple_of(block * BLOCK, BLOCK), BLOCK)
+        for group in range(groups):
+            lanes_x = slice(group * width, (group + 1) * width)
+            lanes_s = slice(group * STATE, (group + 1) * STATE)
             step = fade_scr[group, rows : 2 * rows, at]
             cum, cum_col = cum_scr[group, block], col_scr[group, block]
             x = x_kept[at, lanes_x]
-            c = conv_block(c_pad, c_taps, block, lanes_s).astype(jnp.bfloat16)
-            c_kept[at, lanes_s] = c
+            c = c_kept[at, lanes_s]
             inner = jnp.dot(c, b_kept[group, block], preferred_element_type=jnp.float32)
             mixing = []
             for head in range(per_group):
@@ -329,13 +355,6 @@
                 + readout[:, :width] * spread_heads(fade_in[:, 0:per_group], per_group)
                 + readout[:, width:] * spread_heads(fade_in[:, per_group:rows], per_group)
             )
-            offset = jnp.zeros((1, rows), jnp.float32)
-            for earlier in range(blocks):
-                if earlier < block:
-                    offset = offset + jnp.where(col_at < per_group, totals[earlier], 0.0)
-                if earlier > block:
-                    offset = offset + jnp.where(col_at < per_group, 0.0, totals[earlier])
-            reach_ref[group, at, :] = jnp.exp(cum_col + offset)
 
     def at_level(mask):
         return {"tp": 2 * flip(level, mask, levels) + core}
@@ -349,6 +368,17 @@
             at_level(low_bit(mask, levels)),
         )
 
+    def block_mask(turn):
+        return jnp.where(turn < levels // 2, levels - 1 - 2 * turn, 2 * levels - 2 - 2 * turn)
+
+    woven = 2 * owned == BLOCK and blocks == levels
+    early = min(2, levels) if woven else blocks
+
+    def first_blocks(turn, _):
+        within(flip(level, block_mask(turn), levels) if woven else turn)
+        return 0
+
+    lax.fori_loop(0, early, first_blocks, 0)
     for load in loads:
         load.wait()
     for group in range(groups):
@@ -377,7 +407,7 @@
         post(mask).start()
 
     def one_block(turn, _):
-        mask = jnp.where(turn < levels // 2, levels - 1 - 2 * turn, 2 * levels - 2 - 2 * turn)
+        mask = block_mask(turn)
         at = pl.ds(pl.multiple_of(flip(level, mask, levels) * (2 * owned), 2 * owned), 2 * owned)
         mixed = []
         for group in range(groups):
@@ -407,9 +437,15 @@
         hand(mask).start()
         mine_scr[mask] = full_scr[pl.ds(own, owned), :]
 
-        @pl.when((turn > 0) & (turn <= levels // 2))
+        if woven:
+
+            @pl.when(turn + early < levels)
+            def _():
+                within(flip(level, block_mask(turn + early), levels))
+
+        @pl.when(turn < levels // 2)
         def _():
-            pass_on(levels + 1 - 2 * turn, [])
+            pass_on(mask, [])
 
         return 0
 
@@ -481,11 +517,13 @@
     def column(away):
         return flip(here, away, peers)
 
+    bits = [1 << n for n in range(levels.bit_length() - 1)]
+
     def row_copy(mask):
-        return remote(
-            normed_ref, rows_scr.at[level, core], row_send.at[mask], row_recv.at[mask],
-            at_level(mask),
-        )
+        low = low_bit(mask, levels)
+        spot = rows_scr.at[floor_of(mask - low), core]
+        source = normed_ref if isinstance(mask, int) and mask in bits else spot
+        return remote(source, spot, row_send.at[mask], row_recv.at[mask], at_level(low))
 
     def pair_copy(mask):
         spot = rows_scr.at[floor_of(mask), core]
@@ -527,8 +565,8 @@
         )
 
     rows_scr[level, core] = normed_ref[...]
-    for mask in range(1, levels):
-        row_copy(mask).start()
+    for bit in bits:
+        row_copy(bit).start()
 
     def routes_of(mask):
         floor = floor_of(mask)
@@ -556,6 +594,12 @@
 
     def arrive_and_dispatch(mask):
         row_copy(mask).wait_recv()
+        for bit in bits[:-1]:
+
+            @pl.when(mask % (2 * bit) == 0)
+            def _():
+                row_copy(mask + bit).start()
+
         dispatch(mask)
 
     dispatch(0)
@@ -674,9 +718,9 @@
         hand(mask).start()
         mine_scr[mask] = full_scr[pl.ds(own, owned), :]
 
-        @pl.when(turn > 0)
+        @pl.when(turn < levels - 1)
         def _():
-            pass_on(turn_mask(turn - 1))
+            pass_on(mask)
 
         return 0
 
@@ -734,13 +778,15 @@
         [{"sp": lax.rem(here + away, peers)} for away in range(1, peers)]
         + [{"tp": lax.rem(seat + away, seats)} for away in range(1, seats)]
     )
+    for load in loads[0:3]:
+        load.wait()
     settle = mixer_part(
-        *near, *loaded[0:3], loads[0:3], after_ref, normed_ref, routes, experts_here, share,
+        *loaded[0:3], *near, *loaded[3:6], loads[3:6], after_ref, normed_ref, routes, experts_here, share,
         *mixer_own, *shared, *mixer_flags,
     )
     experts_part(
-        normed_ref, after_ref, routes, out_ref, loads[3:], settle,
-        *experts_own, *shared, *loaded[3:], *experts_flags,
+        normed_ref, after_ref, routes, out_ref, loads[6:], settle,
+        *experts_own, *shared, *loaded[6:], *experts_flags,
     )
 
 
@@ -790,12 +836,12 @@
         return pltpu.SemaphoreType.DMA(shape)
 
     near = [
-        channel_feed_mapped, write_coefficient_mapped, emission_coefficient_mapped,
         channel_feed_taps, write_coefficient_taps, emission_coefficient_taps, raw_increments,
         channel_log_fade_speed, extra_log_fade, picked_specialists.T, router_affinities.T,
         cluster_scaling_factor.reshape(1, -1), routing_scaling_factor.reshape(1, -1),
     ]
     far = [
+        channel_feed_mapped, write_coefficient_mapped, emission_coefficient_mapped,
         result_switch_mapped, skip_stream_entry, blend_result_matrix,
         specialist_switch_matrix, specialist_widen_matrix, specialist_contract_matrix,
     ]

time: 133 us -> 124 us (0.932)
  Pallas kernels: 129 us -> 121 us
    pallas_call x1, Pallas kernels: 129 us -> 121 us  [per_device(): pl.pallas_call(functools.partial(layer_kernel, experts_here, share, (len(...]
where the time goes in v2:
time: 124 us; the launch traced here: 123 us
  Pallas kernels  121 us (98%)
  other arithmetic  1.77 us (1%)
    pallas_call x1, Pallas kernels, per_device(): pl.pallas_call(functools.partial(layer_kernel, experts_here, share, (len(...  121 us

profile of v2, /device:TPU:17, one launch (start us, length us, event | category | flops | bytes accessed | tf_op | source)
XLA Modules:
  0.0 122.8 jit_solution(14585041554296265646)
XLA Ops:
  0.0 121.0 %layer.1 = f32[64,2048]{1,0:T(8,128)} custom-call(bf16[5,512]{1,0:T(8,128)(2,1)} %refs_0_.1, bf16[5,256]{1,0:T(8,128)(2,1)} %refs_1_.1, bf16[5,256]{1,0:T(8,128)(2,1)} %refs_2_.1, bf16[2,8,512]{2,1,0:T(8,128)(2,1)} %refs_3_.1, f32[2,8]{1,0:T(2,128)} %refs_4_.1, f32[2,8,512]{2,1,0:T(8,128)} %refs_5_.1, s32[2,64]{1,0:T(2,128)} %bitcast.6, f32[2,64]{1,0:T(2,128)} %bitcast.7, ...), custom_call_target="tpu_custom_call" | custom-call | tf_op jit(solution)/shard_map/layer/pallas_call | solution.py:882
  121.0 1.8 %convert_element_type.3 = bf16[64,2048]{1,0:T(8,128)(2,1)} convert(f32[64,2048]{1,0:T(8,128)} %layer.1) | non-fusion elementwise | flops 131072 | bytes 786432 | tf_op jit(solution)/shard_map/convert_element_type | solution.py:894

commit v3 on v2

--- a/solution.py
+++ b/solution.py
@@ -189,46 +189,12 @@
             spot = first * per_group
             fade_scr[group, spot : spot + per_group, :] = fade[mine, :]
             fade_scr[group, rows + spot : rows + spot + per_group, :] = step[mine, :]
-    for pad, source in ((x_pad, x_ref), (b_pad, b_ref), (c_pad, c_ref)):
-        pad[RIM : RIM + count, :] = source[...].astype(jnp.float32)
-
-    @pl.when(here > 0)
-    def _():
-        for onward, _ in edges:
-            onward.wait_recv()
-        for pad, low in ((x_pad, x_low), (b_pad, b_low), (c_pad, c_low)):
-            pad[RIM - rim : RIM, :] = low[...].astype(jnp.float32)[EDGE - rim : EDGE, :]
-
-    @pl.when(here == 0)
-    def _():
-        for pad in (x_pad, b_pad, c_pad):
-            pad[RIM - rim : RIM, :] = jnp.zeros((rim, pad.shape[1]), jnp.float32)
-
-    @pl.when(here < peers - 1)
-    def _():
-        for _, back in edges:
-            back.wait_recv()
-        for pad, high in ((x_pad, x_high), (b_pad, b_high), (c_pad, c_high)):
-            pad[RIM + count : RIM + count + rim, :] = high[...].astype(jnp.float32)[0:rim, :]
-
-    @pl.when(here == peers - 1)
-    def _():
-        for pad in (x_pad, b_pad, c_pad):
-            pad[RIM + count : RIM + count + rim, :] = jnp.zeros((rim, pad.shape[1]), jnp.float32)
-
     i_at = lax.broadcasted_iota(jnp.int32, (BLOCK, BLOCK), 0)
     j_at = lax.broadcasted_iota(jnp.int32, (BLOCK, BLOCK), 1)
     up_to = (i_at <= j_at).astype(jnp.float32)
     from_on = (i_at >= j_at).astype(jnp.float32)
     col_at = lax.broadcasted_iota(jnp.int32, (1, rows), 1)
     half_lane = lax.broadcasted_iota(jnp.int32, (BLOCK, 2 * HEAD_DIM), 1) < HEAD_DIM
-
-    def state_copy(group, away):
-        peer = lax.rem(here + away, peers)
-        return remote(
-            state_ref.at[jnp.where(peer > here, 0, 1), group], target.at[here, group],
-            state_send.at[group, away - 1], state_recv.at[group, away - 1], {"sp": peer},
-        )
 
     spots = [(group, block) for group in range(groups) for block in range(blocks)]
     fades = jnp.concatenate(
@@ -254,6 +220,40 @@
             columns[spot] = (
                 turned[:, lane : lane + rows], turned[:, lane + rows : lane + 2 * rows]
             )
+
+    for pad, source in ((x_pad, x_ref), (b_pad, b_ref), (c_pad, c_ref)):
+        pad[RIM : RIM + count, :] = source[...].astype(jnp.float32)
+
+    @pl.when(here > 0)
+    def _():
+        for onward, _ in edges:
+            onward.wait_recv()
+        for pad, low in ((x_pad, x_low), (b_pad, b_low), (c_pad, c_low)):
+            pad[RIM - rim : RIM, :] = low[...].astype(jnp.float32)[EDGE - rim : EDGE, :]
+
+    @pl.when(here == 0)
+    def _():
+        for pad in (x_pad, b_pad, c_pad):
+            pad[RIM - rim : RIM, :] = jnp.zeros((rim, pad.shape[1]), jnp.float32)
+
+    @pl.when(here < peers - 1)
+    def _():
+        for _, back in edges:
+            back.wait_recv()
+        for pad, high in ((x_pad, x_high), (b_pad, b_high), (c_pad, c_high)):
+            pad[RIM + count : RIM + count + rim, :] = high[...].astype(jnp.float32)[0:rim, :]
+
+    @pl.when(here == peers - 1)
+    def _():
+        for pad in (x_pad, b_pad, c_pad):
+            pad[RIM + count : RIM + count + rim, :] = jnp.zeros((rim, pad.shape[1]), jnp.float32)
+
+    def state_copy(group, away):
+        peer = flip(here, peers - away, peers)
+        return remote(
+            state_ref.at[jnp.where(peer > here, 0, 1), group], target.at[here, group],
+            state_send.at[group, away - 1], state_recv.at[group, away - 1], {"sp": peer},
+        )
 
     all_totals = []
     for group in range(groups):
@@ -705,18 +705,20 @@
         low = (weight - high.astype(jnp.float32)).astype(jnp.bfloat16)
         for away in away_order:
             back_copy(mask, away).wait_recv()
-        width = min(512, features)
-        for start in range(0, features, width):
-            lanes = slice(start, start + width)
-            got = returned[floor_of(mask), :, :, lanes].reshape(slots, width)
-            full_scr[:, lanes] = jnp.dot(
-                high, got, preferred_element_type=jnp.float32
-            ) + jnp.dot(low, got, preferred_element_type=jnp.float32)
-        own = pl.multiple_of(core * owned, owned)
-        other = pl.multiple_of((1 - core) * owned, owned)
-        give[mask] = full_scr[pl.ds(other, owned), :].astype(jnp.bfloat16)
+        first_high, second_high = high[0:owned, :], high[owned:, :]
+        first_low, second_low = low[0:owned, :], low[owned:, :]
+
+        def product(pick):
+            top = jnp.where(pick == 0, first_high, second_high)
+            rest = jnp.where(pick == 0, first_low, second_low)
+            got = returned[floor_of(mask)].reshape(slots, features)
+            return jnp.dot(top, got, preferred_element_type=jnp.float32) + jnp.dot(
+                rest, got, preferred_element_type=jnp.float32
+            )
+
+        give[mask] = product(1 - core).astype(jnp.bfloat16)
         hand(mask).start()
-        mine_scr[mask] = full_scr[pl.ds(own, owned), :]
+        mine_scr[mask] = product(core)
 
         @pl.when(turn < levels - 1)
         def _():
@@ -770,7 +772,7 @@
         pltpu.make_async_copy(source, target, load_sem.at[index])
         for index, (source, target) in enumerate(zip(far, loaded))
     ]
-    for load in loads:
+    for load in loads[0:3]:
         load.start()
     here, peers = lax.axis_index("sp"), lax.axis_size("sp")
     seat, seats = lax.axis_index("tp"), lax.axis_size("tp")
@@ -780,6 +782,8 @@
     )
     for load in loads[0:3]:
         load.wait()
+    for load in loads[3:]:
+        load.start()
     settle = mixer_part(
         *loaded[0:3], *near, *loaded[3:6], loads[3:6], after_ref, normed_ref, routes, experts_here, share,
         *mixer_own, *shared, *mixer_flags,

time: 124 us -> 124 us (level)
  no operation moved by 1% of the time
where the time goes in v3:
time: 124 us; the launch traced here: 123 us
  Pallas kernels  121 us (98%)
  other arithmetic  1.77 us (1%)
    pallas_call x1, Pallas kernels, per_device(): pl.pallas_call(functools.partial(layer_kernel, experts_here, share, (len(...  121 us

profile of v3, /device:TPU:17, one launch (start us, length us, event | category | flops | bytes accessed | tf_op | source)
XLA Modules:
  0.0 122.5 jit_solution(16702606738457167863)
XLA Ops:
  0.0 120.7 %layer.1 = f32[64,2048]{1,0:T(8,128)} custom-call(bf16[5,512]{1,0:T(8,128)(2,1)} %refs_0_.1, bf16[5,256]{1,0:T(8,128)(2,1)} %refs_1_.1, bf16[5,256]{1,0:T(8,128)(2,1)} %refs_2_.1, bf16[2,8,512]{2,1,0:T(8,128)(2,1)} %refs_3_.1, f32[2,8]{1,0:T(2,128)} %refs_4_.1, f32[2,8,512]{2,1,0:T(8,128)} %refs_5_.1, s32[2,64]{1,0:T(2,128)} %bitcast.6, f32[2,64]{1,0:T(2,128)} %bitcast.7, ...), custom_call_target="tpu_custom_call" | custom-call | tf_op jit(solution)/shard_map/layer/pallas_call | solution.py:886
  120.7 1.8 %convert_element_type.3 = bf16[64,2048]{1,0:T(8,128)(2,1)} convert(f32[64,2048]{1,0:T(8,128)} %layer.1) | non-fusion elementwise | flops 131072 | bytes 786432 | tf_op jit(solution)/shard_map/convert_element_type | solution.py:898
